TPU v7x, 32 devices: a whole 2x2x4 slice. The times are simulated.
32 devices in a mesh: grp: 2 (over x), ep: 8 (over z, y), tp: 2 (over core).
Axes of the slice: x: 2, y: 2, z: 4, core: 2. Of those that a mesh axis runs over, the one named last changes fastest.
Arguments:
- tokens: bfloat16 [8192, 2048], P(('grp', 'ep', 'tp')), parts along dimension 0, may hold values from -6 to 6
- norm_gain: float32 [2048], replicated, may hold values from 0.1 to 1.9
- routes: int32 [8192, 3], P(('grp', 'ep', 'tp')), parts along dimension 0, may hold values from 0 to 7, all different within a row; in each aligned block of 256 rows (0 to 255, 256 to 511, ...) at most 144 rows name the same one
- gates: float32 [8192, 3], P(('grp', 'ep', 'tp')), parts along dimension 0, may hold values from 0.2 to 1.2
- expert_gate: bfloat16 [8, 2048, 512], P('ep', None, 'tp'), may hold values from -0.125 to 0.125
- expert_up: bfloat16 [8, 2048, 512], P('ep', None, 'tp'), may hold values from -0.125 to 0.125
- expert_down: bfloat16 [8, 512, 2048], P('ep', 'tp'), may hold values from -0.25 to 0.25
- shared_gate: bfloat16 [2048, 512], replicated, may hold values from -0.125 to 0.125
- shared_up: bfloat16 [2048, 512], replicated, may hold values from -0.125 to 0.125
- shared_down: bfloat16 [512, 2048], replicated, may hold values from -0.25 to 0.25
Outputs:
- mixed: bfloat16 [8192, 2048], P(('grp', 'ep', 'tp')), parts along dimension 0
There are 2 independent parts, one for each index of `grp`. A program takes and returns all parts, laid end to end along the dimension named above; an argument that names none is the same for every part. Nothing has to cross between parts.
Inputs may be any that keep to these rules, and one draw needn't show every extreme that they name: `routes`: A row names 3 different experts. Among the rows of one device no expert is named by more than 144 rows, and in every draw some expert is named by exactly 144 rows of some device.
All inputs are finite; a program needn't handle non-finite values.
Results may differ from a plain program's by a relative error of at most 0.01.
Values may be sent and summed in bfloat16 or wider, within the bound.
No kernel may reach another device: no remote copies, remote signals or barrier semaphores. Data moves between devices by JAX's collectives and lax.ppermute only.
A program may use at most 128 MiB of HBM per device.

v0:
```python
import functools

import jax
import jax.numpy as jnp
from jax import lax
from jax.experimental import pallas as pl
from jax.experimental.pallas import tpu as pltpu
from jax.sharding import PartitionSpec as P

F32 = jnp.float32
BF16 = jnp.bfloat16


def dot(a, b):
    return jnp.dot(a, b, preferred_element_type=F32)


def slots_of(routes, first, count, capacity):
    rows = routes.shape[0]
    names = first + jnp.arange(count, dtype=jnp.int32)
    member = jnp.any(routes[:, :, None] == names[None, None, :], axis=1)
    before = jnp.arange(rows)[:, None] > jnp.arange(rows)[None, :]
    rank = dot(before.astype(BF16), member.astype(BF16)).astype(jnp.int32)
    rank = jnp.where(member, rank, -1).T
    onehot = rank[:, None, :] == jnp.arange(capacity, dtype=jnp.int32)[None, :, None]
    return onehot.reshape(count * capacity, rows)


def weights_of(onehot, routes, gates, first, count, capacity):
    names = first + jnp.arange(count, dtype=jnp.int32)
    chosen = routes[:, :, None] == names[None, None, :]
    scale = jnp.sum(jnp.where(chosen, gates[:, :, None], 0.0), axis=1).T
    wide = jnp.repeat(scale.astype(BF16), capacity, axis=0)
    return jnp.where(onehot, wide, jnp.zeros((), BF16))


def combine(weights, back):
    dims = (((0,), (0,)), ((), ()))
    return lax.dot_general(weights, back, dims, preferred_element_type=F32)


def expert_kernel(*refs, parts):
    x_ref, out_ref = refs[0], refs[-1]
    x = x_ref[...]
    hidden = []
    for p in range(parts):
        gate = dot(x, refs[1 + p][...])
        up = dot(x, refs[1 + parts + p][...])
        hidden.append((jax.nn.silu(gate) * up).astype(BF16))
    width = out_ref.shape[1]
    step = 256 if width % 256 == 0 else width
    for at in range(0, width, step):
        total = None
        for p in range(parts):
            piece = dot(hidden[p], refs[1 + 2 * parts + p][:, at : at + step])
            total = piece if total is None else total + piece
        out_ref[:, at : at + step] = total.astype(BF16)


def expert(x, gate_parts, up_parts, down_parts):
    parts = len(gate_parts)
    rows, width = x.shape
    units = gate_parts[0].shape[1]
    operands = [x, *gate_parts, *up_parts, *down_parts]
    return pl.pallas_call(
        functools.partial(expert_kernel, parts=parts),
        out_shape=jax.ShapeDtypeStruct((rows, width), BF16),
        in_specs=[pl.BlockSpec(memory_space=pltpu.VMEM)] * len(operands),
        out_specs=pl.BlockSpec(memory_space=pltpu.VMEM),
        cost_estimate=pl.CostEstimate(
            flops=6 * rows * width * units * parts,
            bytes_accessed=4 * rows * width + 6 * parts * width * units,
            transcendentals=rows * units * parts,
        ),
        compiler_params=pltpu.CompilerParams(vmem_limit_bytes=40 * 1024 * 1024),
        name="expert",
    )(*operands)


def on_device(
    tokens,
    norm_gain,
    routes,
    gates,
    expert_gate,
    expert_up,
    expert_down,
    shared_gate,
    shared_up,
    shared_down,
):
    rows, width = tokens.shape
    top = routes.shape[1]
    local = expert_gate.shape[0]
    groups = lax.axis_size("ep")
    cores = lax.axis_size("tp")
    experts = local * groups
    capacity = 3 * rows * top // (2 * experts)
    half = groups // 2
    mine = experts // 2
    first = (lax.axis_index("ep") // half) * mine
    halves = [list(range(half)), list(range(half, groups))]
    across = [(i, (i + half) % groups) for i in range(groups)]

    values = tokens.astype(F32)
    scaling = lax.rsqrt(jnp.mean(values * values, axis=1, keepdims=True) + 1e-06)
    normed = (values * scaling * norm_gain[None, :]).astype(BF16)

    far_normed = lax.ppermute(normed, "ep", across)
    table = jnp.concatenate([routes.astype(F32), gates], axis=1)
    far_table = lax.ppermute(table, "ep", across)
    far_routes = far_table[:, :top].astype(jnp.int32)
    far_gates = far_table[:, top:]

    gate_parts, up_parts, down_parts = [expert_gate], [expert_up], [expert_down]
    for shift in range(1, cores):
        ring = [(i, (i + shift) % cores) for i in range(cores)]
        gate_parts.append(lax.ppermute(expert_gate, "tp", ring))
        up_parts.append(lax.ppermute(expert_up, "tp", ring))
        down_parts.append(lax.ppermute(expert_down, "tp", ring))

    def exchange(array):
        return lax.all_to_all(
            array, "ep", split_axis=0, concat_axis=0, tiled=True, axis_index_groups=halves
        )

    def send(onehot, source):
        picked = dot(onehot.astype(BF16), source).astype(BF16)
        return exchange(picked.reshape(half, local, capacity, width))

    def run(received):
        outs = []
        for e in range(local):
            x = received[:, e].reshape(half * capacity, width)
            weights = ([part[e] for part in kind] for kind in (gate_parts, up_parts, down_parts))
            outs.append(expert(x, *weights).reshape(half, capacity, width))
        return jnp.stack(outs, axis=1)

    near_slots = slots_of(routes, first, mine, capacity)
    near_in = send(near_slots, normed)

    shared_hidden = (
        jax.nn.silu(dot(normed, shared_gate)) * dot(normed, shared_up)
    ).astype(BF16)
    shared_out = dot(shared_hidden, shared_down)
    far_slots = slots_of(far_routes, first, mine, capacity).astype(BF16)
    far_normed, near_in, shared_out, far_slots, far_gates, gate_parts, up_parts, down_parts = (
        lax.optimization_barrier(
            (far_normed, near_in, shared_out, far_slots, far_gates, gate_parts, up_parts, down_parts)
        )
    )
    far_in = send(far_slots, far_normed)
    near_done = run(near_in)
    near_weights = weights_of(near_slots, routes, gates, first, mine, capacity)
    far_weights = weights_of(far_slots > 0, far_routes, far_gates, first, mine, capacity)
    far_in, near_done = lax.optimization_barrier((far_in, near_done))
    far_back = exchange(run(far_in))
    far_back, near_done = lax.optimization_barrier((far_back, near_done))
    near_back = exchange(near_done).reshape(mine * capacity, width)
    far_sum = combine(far_weights, far_back.reshape(mine * capacity, width))
    home = lax.ppermute(far_sum.astype(BF16), "ep", across)
    near_back, home = lax.optimization_barrier((near_back, home))
    return (combine(near_weights, near_back) + (shared_out + home.astype(F32))).astype(BF16)


def solution(mesh):
    return jax.shard_map(
        on_device,
        mesh=mesh,
        in_specs=(
            P(("grp", "ep", "tp"), None),
            P(),
            P(("grp", "ep", "tp"), None),
            P(("grp", "ep", "tp"), None),
            P("ep", None, "tp"),
            P("ep", None, "tp"),
            P("ep", "tp", None),
            P(),
            P(),
            P(),
        ),
        out_specs=P(("grp", "ep", "tp"), None),
        check_vma=False,
    )
```

profile of v0, /device:TPU:0, one launch (start us, length us, event | category | flops | bytes accessed | tf_op | source)
XLA Modules:
  0.0 200.8 jit_solution(272638794600694932)
XLA Ops:
  0.0 0.0 copy-start
  0.0 0.0 copy-start.8
  0.0 0.9 convert_element_type.65
  0.9 0.7 pad_maximum_fusion
  1.6 4.1 %collective-permute-start.1 = (f32[256,6]{0,1:T(8,128)S(1)}, f32[256,6]{0,1:T(8,128)S(1)}, u32[]{:S(2)}, u32[]{:S(2)}) collective-permute-start(f32[256,6]{0,1:T(8,128)S(1)} %pad_maximum_fusion), channel_id=1, source_target_pairs={{0,8},{2,10},{4,12},{6,14},{8,0},{10,2},{12,4},{14,6},{1,9},{3,11}... | collective-permute-start | bytes 18440 | tf_op jit(solution)/shard_map/ppermute | solution.py:111
  5.6 1.5 fusion.1
  7.2 1.5 fusion.3
  8.7 0.0 copy-start.7
  8.7 0.1 eq.84
  8.8 0.0 collective-permute-done.1
  8.8 0.0 copy-done.8
  8.8 0.1 compare_reduce_fusion
  8.9 0.2 fusion.6
  9.1 0.2 fusion.7
  9.3 0.2 fusion.8
  9.5 2.2 %convolution_convert_fusion.1 = bf16[576,2048]{1,0:T(8,128)(2,1)} fusion(pred[576,256]{1,0:T(32,128)(4,1)S(1)} %get-tuple-element.46, bf16[256,2048]{1,0:T(8,128)(2,1)S(1)} %fusion.3), kind=kOutput, calls=%fused_computation.1 | convolution fusion | flops 605159424 | bytes 3555328 | tf_op jit(solution)/shard_map/dot_general | solution.py:15
  11.7 0.0 copy-done.7
  11.7 0.0 copy-start.2
  11.7 4.6 %all-to-all-start = ((bf16[4,1,144,2048]{3,2,1,0:T(8,128)(2,1)}), bf16[4,1,144,2048]{3,2,1,0:T(8,128)(2,1)}, u32[]{:S(2)}, u32[]{:S(2)}) async-start(bf16[4,1,144,2048]{3,2,1,0:T(8,128)(2,1)} %bitcast.64), calls=%async_computation | async-start | bytes 4718592 | tf_op jit(solution)/shard_map/all_to_all | solution.py:123
  16.3 1.4 collective-permute-start
  17.7 0.0 copy-done.2
  17.7 0.0 collective-permute-start.2
  17.7 0.5 collective-permute-start.3
  18.2 0.0 collective-permute-start.4
  18.2 3.4 %fusion.21 = f32[256,512]{1,0:T(8,128)} fusion(bf16[256,2048]{1,0:T(8,128)(2,1)} %copy-done.7, bf16[2048,512]{1,0:T(8,128)(2,1)} %param.17), kind=kOutput, calls=%fused_computation.45 | convolution fusion | flops 536870912 | bytes 3670016 | tf_op jit(solution)/shard_map/dot_general | solution.py:15
  21.7 0.0 copy-done
  21.7 4.7 %fusion.5 = f32[256,2048]{1,0:T(8,128)} fusion(bf16[512,2048]{1,0:T(8,128)(2,1)S(1)} %copy-done, bf16[256,2048]{1,0:T(8,128)(2,1)} %copy-done.7, bf16[2048,512]{1,0:T(8,128)(2,1)} %param.18, f32[256,512]{1,0:T(8,128)} %fusion.21), kind=kOutput, calls=%fused_computation.12 | convolution fusion | flops 1074528256 | bytes 7864320 | tf_op jit(solution)/shard_map/dot_general | solution.py:15
  26.4 38.0 %collective-permute-done = bf16[256,2048]{1,0:T(8,128)(2,1)} collective-permute-done((bf16[256,2048]{1,0:T(8,128)(2,1)}, bf16[256,2048]{1,0:T(8,128)(2,1)}, u32[]{:S(2)}, u32[]{:S(2)}) %collective-permute-start) | collective-permute-done | bytes 1048608 | tf_op jit(solution)/shard_map/ppermute | solution.py:109
  64.4 0.0 collective-permute-done.2
  64.4 0.0 collective-permute-done.3
  64.4 0.0 collective-permute-done.4
  64.4 2.2 %all-to-all-done = bf16[4,1,144,2048]{3,2,1,0:T(8,128)(2,1)} async-done(((bf16[4,1,144,2048]{3,2,1,0:T(8,128)(2,1)}), bf16[4,1,144,2048]{3,2,1,0:T(8,128)(2,1)}, u32[]{:S(2)}, u32[]{:S(2)}) %all-to-all-start) | async-done | bytes 2359328 | tf_op jit(solution)/shard_map/all_to_all | solution.py:123
  66.5 3.4 %convolution_convert_fusion = bf16[576,2048]{1,0:T(8,128)(2,1)} fusion(bf16[576,256]{1,0:T(8,128)(2,1)S(1)} %get-tuple-element.22, bf16[256,2048]{1,0:T(8,128)(2,1)} %collective-permute-done), kind=kOutput, calls=%fused_computation | convolution fusion | flops 605159424 | bytes 3702784 | tf_op jit(solution)/shard_map/dot_general | solution.py:15
  70.0 4.5 %all-to-all-start.1 = ((bf16[4,1,144,2048]{3,2,1,0:T(8,128)(2,1)}), bf16[4,1,144,2048]{3,2,1,0:T(8,128)(2,1)}, u32[]{:S(2)}, u32[]{:S(2)}) async-start(bf16[4,1,144,2048]{3,2,1,0:T(8,128)(2,1)} %bitcast.65), calls=%async_computation.1 | async-start | bytes 4718592 | tf_op jit(solution)/shard_map/all_to_all | solution.py:123
  74.5 0.0 copy-start.3
  74.5 1.2 copy-done.3
  75.7 0.0 copy-start.5
  75.7 1.2 copy-done.5
  76.9 6.4 %expert.2 = bf16[576,2048]{1,0:T(8,128)(2,1)S(1)} custom-call(bf16[576,2048]{1,0:T(8,128)(2,1)} %bitcast.10.refs_0_, bf16[2048,256]{1,0:T(8,128)(2,1)S(1)} %bitcast.58, bf16[2048,256]{1,0:T(8,128)(2,1)} %bitcast.12.refs_2_, bf16[2048,256]{1,0:T(8,128)(2,1)S(1)} %bitcast.60, bf16[2048,256]{1,0:T(8,128)(2,1)} %bitcast.14.refs_4_, ...), custom_call_target="tpu_custom_call" | custom-call | flops 3623878656 | bytes 11010048 | tf_op jit(solution)/shard_map/expert/pallas_call | solution.py:65
  83.3 0.0 copy-start.1
  83.3 1.4 copy-done.1
  84.7 17.0 %all-to-all-done.1 = bf16[4,1,144,2048]{3,2,1,0:T(8,128)(2,1)} async-done(((bf16[4,1,144,2048]{3,2,1,0:T(8,128)(2,1)}), bf16[4,1,144,2048]{3,2,1,0:T(8,128)(2,1)}, u32[]{:S(2)}, u32[]{:S(2)}) %all-to-all-start.1) | async-done | bytes 2359328 | tf_op jit(solution)/shard_map/all_to_all | solution.py:123
  101.7 0.0 copy-start.4
  101.7 1.2 copy-done.4
  102.9 0.0 copy-start.6
  102.9 1.2 copy-done.6
  104.2 6.4 %expert.3 = bf16[576,2048]{1,0:T(8,128)(2,1)S(1)} custom-call(bf16[576,2048]{1,0:T(8,128)(2,1)} %bitcast.18.refs_0_, bf16[2048,256]{1,0:T(8,128)(2,1)S(1)} %bitcast.59, bf16[2048,256]{1,0:T(8,128)(2,1)} %bitcast.12.refs_2_, bf16[2048,256]{1,0:T(8,128)(2,1)S(1)} %bitcast.61, bf16[2048,256]{1,0:T(8,128)(2,1)} %bitcast.14.refs_4_, ...), custom_call_target="tpu_custom_call" | custom-call | flops 3623878656 | bytes 11010048 | tf_op jit(solution)/shard_map/expert/pallas_call | solution.py:65
  110.6 31.1 %all_to_all.20 = bf16[4,1,144,2048]{3,2,1,0:T(8,128)(2,1)} all-to-all(bf16[4,1,144,2048]{3,2,1,0:T(8,128)(2,1)S(1)} %bitcast.57), channel_id=1, replica_groups={{0,2,4,6},{8,10,12,14},{1,3,5,7},{9,11,13,15},{16,18,20,22},{24,26,28,3..., dimensions={0} | all-to-all | bytes 4718592 | tf_op jit(solution)/shard_map/all_to_all | solution.py:123
  141.6 0.0 copy-start.9
  141.6 4.6 %all-to-all-start.3 = ((bf16[4,1,144,2048]{3,2,1,0:T(8,128)(2,1)}), bf16[4,1,144,2048]{3,2,1,0:T(8,128)(2,1)}, u32[]{:S(2)}, u32[]{:S(2)}) async-start(bf16[4,1,144,2048]{3,2,1,0:T(8,128)(2,1)} %bitcast.56), calls=%async_computation.3 | async-start | bytes 4718592 | tf_op jit(solution)/shard_map/all_to_all | solution.py:123
  146.3 0.0 copy-done.9
  146.3 0.1 fusion.17
  146.4 2.7 %convolution_convert_fusion.2 = bf16[256,2048]{1,0:T(8,128)(2,1)S(1)} fusion(bf16[576,2048]{1,0:T(8,128)(2,1)} %bitcast.66, bf16[576,256]{1,0:T(8,128)(2,1)S(1)} %bitcast.67, bf16[576,256]{1,0:T(8,128)(2,1)S(1)} %get-tuple-element.22), kind=kOutput, calls=%fused_computation.5 | convolution fusion | flops 604798976 | bytes 3997696 | tf_op jit(solution)/shard_map/dot_general | solution.py:39
  149.1 1.2 collective-permute-start.5
  150.3 0.1 bitcast_select_fusion
  150.5 46.0 %collective-permute-done.5 = bf16[256,2048]{1,0:T(8,128)(2,1)S(1)} collective-permute-done((bf16[256,2048]{1,0:T(8,128)(2,1)S(1)}, bf16[256,2048]{1,0:T(8,128)(2,1)S(1)}, u32[]{:S(2)}, u32[]{:S(2)}) %collective-permute-start.5) | collective-permute-done | bytes 1048608 | tf_op jit(solution)/shard_map/ppermute | solution.py:161
  196.5 0.0 all-to-all-done.3
  196.5 4.3 %fusion = bf16[256,2048]{1,0:T(8,128)(2,1)} fusion(bf16[576,256]{1,0:T(8,128)(2,1)S(1)} %bitcast_select_fusion, bf16[576,2048]{1,0:T(8,128)(2,1)} %bitcast.22, f32[256,2048]{1,0:T(8,128)} %fusion.5, bf16[256,2048]{1,0:T(8,128)(2,1)S(1)} %collective-permute-done.5), kind=kOutput, calls=%fused_computation.6 | convolution fusion | flops 606076928 | bytes 6848512 | tf_op jit(solution)/shard_map/dot_general | solution.py:39
  (5 shorter events, 0.1 us)
Async XLA Ops:
  0.0 21.7 %copy-start = (bf16[512,2048]{1,0:T(8,128)(2,1)S(1)}, bf16[512,2048]{1,0:T(8,128)(2,1)}, u32[]{:S(2)}) copy-start(bf16[512,2048]{1,0:T(8,128)(2,1)} %param.19) | copy-start | bytes 6291460
  0.0 8.8 %copy-start.8 = (s32[256,3]{0,1:T(4,128)S(1)}, s32[256,3]{0,1:T(4,128)}, u32[]{:S(2)}) copy-start(s32[256,3]{0,1:T(4,128)} %param.12) | copy-start | bytes 9220
  1.6 7.3 %collective-permute-start.1 = (f32[256,6]{0,1:T(8,128)S(1)}, f32[256,6]{0,1:T(8,128)S(1)}, u32[]{:S(2)}, u32[]{:S(2)}) collective-permute-start(f32[256,6]{0,1:T(8,128)S(1)} %pad_maximum_fusion), channel_id=1, source_target_pairs={{0,8},{2,10},{4,12},{6,14},{8,0},{10,2},{12,4},{14,6},{1,9},{3,11}... | collective-permute-start | bytes 18440 | tf_op jit(solution)/shard_map/ppermute | solution.py:111
  8.7 3.0 %copy-start.7 = (bf16[256,2048]{1,0:T(8,128)(2,1)}, bf16[256,2048]{1,0:T(8,128)(2,1)S(1)}, u32[]{:S(2)}) copy-start(bf16[256,2048]{1,0:T(8,128)(2,1)S(1)} %fusion.3) | copy-start | bytes 3145732
  11.7 6.0 %copy-start.2 = (bf16[1,2048,256]{2,1,0:T(8,128)(2,1)S(1)}, bf16[1,2048,256]{2,1,0:T(8,128)(2,1)}, u32[]{:S(2)}) copy-start(bf16[1,2048,256]{2,1,0:T(8,128)(2,1)} %param.14) | copy-start | bytes 3145732
  11.7 54.8 %all-to-all-start = ((bf16[4,1,144,2048]{3,2,1,0:T(8,128)(2,1)}), bf16[4,1,144,2048]{3,2,1,0:T(8,128)(2,1)}, u32[]{:S(2)}, u32[]{:S(2)}) async-start(bf16[4,1,144,2048]{3,2,1,0:T(8,128)(2,1)} %bitcast.64), calls=%async_computation | async-start | bytes 4718592 | tf_op jit(solution)/shard_map/all_to_all | solution.py:123
  16.3 48.0 %collective-permute-start = (bf16[256,2048]{1,0:T(8,128)(2,1)}, bf16[256,2048]{1,0:T(8,128)(2,1)}, u32[]{:S(2)}, u32[]{:S(2)}) collective-permute-start(bf16[256,2048]{1,0:T(8,128)(2,1)} %copy-done.7), channel_id=1, source_target_pairs={{0,8},{2,10},{4,12},{6,14},{8,0},{10,2},{12,4},{14,6},{1,9},{3,11}... | collective-permute-start | bytes 3145736 | tf_op jit(solution)/shard_map/ppermute | solution.py:109
  17.7 46.6 %collective-permute-start.2 = (bf16[1,2048,256]{2,1,0:T(8,128)(2,1)S(1)}, bf16[1,2048,256]{2,1,0:T(8,128)(2,1)}, u32[]{:S(2)}, u32[]{:S(2)}) collective-permute-start(bf16[1,2048,256]{2,1,0:T(8,128)(2,1)S(1)} %copy-done.2), channel_id=1, source_target_pairs={{0,1},{1,0},{2,3},{3,2},{4,5},{5,4},{6,7},{7,6},{8,9},{9,8},{10,11... | collective-permute-start | bytes 3145736 | tf_op jit(solution)/shard_map/ppermute | solution.py:118
  17.7 46.6 %collective-permute-start.3 = (bf16[1,2048,256]{2,1,0:T(8,128)(2,1)}, bf16[1,2048,256]{2,1,0:T(8,128)(2,1)}, u32[]{:S(2)}, u32[]{:S(2)}) collective-permute-start(bf16[1,2048,256]{2,1,0:T(8,128)(2,1)} %param.15), channel_id=1, source_target_pairs={{0,1},{1,0},{2,3},{3,2},{4,5},{5,4},{6,7},{7,6},{8,9},{9,8},{10,11... | collective-permute-start | bytes 3145736 | tf_op jit(solution)/shard_map/ppermute | solution.py:119
  18.2 46.1 %collective-permute-start.4 = (bf16[1,256,2048]{2,1,0:T(8,128)(2,1)}, bf16[1,256,2048]{2,1,0:T(8,128)(2,1)}, u32[]{:S(2)}, u32[]{:S(2)}) collective-permute-start(bf16[1,256,2048]{2,1,0:T(8,128)(2,1)} %param.16), channel_id=1, source_target_pairs={{0,1},{1,0},{2,3},{3,2},{4,5},{5,4},{6,7},{7,6},{8,9},{9,8},{10,11... | collective-permute-start | bytes 3145736 | tf_op jit(solution)/shard_map/ppermute | solution.py:120
  70.0 31.8 %all-to-all-start.1 = ((bf16[4,1,144,2048]{3,2,1,0:T(8,128)(2,1)}), bf16[4,1,144,2048]{3,2,1,0:T(8,128)(2,1)}, u32[]{:S(2)}, u32[]{:S(2)}) async-start(bf16[4,1,144,2048]{3,2,1,0:T(8,128)(2,1)} %bitcast.65), calls=%async_computation.1 | async-start | bytes 4718592 | tf_op jit(solution)/shard_map/all_to_all | solution.py:123
  74.5 1.2 copy-start.3
  75.7 1.2 copy-start.5
  83.3 1.4 copy-start.1
  101.7 1.2 copy-start.4
  102.9 1.2 copy-start.6
  141.6 4.7 %copy-start.9 = (f32[256,3]{0,1:T(4,128)S(1)}, f32[256,3]{0,1:T(4,128)}, u32[]{:S(2)}) copy-start(f32[256,3]{0,1:T(4,128)} %param.13) | copy-start | bytes 9220
  141.6 54.9 %all-to-all-start.3 = ((bf16[4,1,144,2048]{3,2,1,0:T(8,128)(2,1)}), bf16[4,1,144,2048]{3,2,1,0:T(8,128)(2,1)}, u32[]{:S(2)}, u32[]{:S(2)}) async-start(bf16[4,1,144,2048]{3,2,1,0:T(8,128)(2,1)} %bitcast.56), calls=%async_computation.3 | async-start | bytes 4718592 | tf_op jit(solution)/shard_map/all_to_all | solution.py:123
  149.1 47.4 %collective-permute-start.5 = (bf16[256,2048]{1,0:T(8,128)(2,1)S(1)}, bf16[256,2048]{1,0:T(8,128)(2,1)S(1)}, u32[]{:S(2)}, u32[]{:S(2)}) collective-permute-start(bf16[256,2048]{1,0:T(8,128)(2,1)S(1)} %convolution_convert_fusion.2), channel_id=1, source_target_pairs={{0,8},{2,10},{4,12},{6,14},{8,0},{10,2},{12,4},{14,6},{1,9},{3,11}... | collective-permute-start | bytes 3145736 | tf_op jit(solution)/shard_map/ppermute | solution.py:161
where the time goes:
time: 202 us; the launch traced here: 201 us
  waiting for transfers between devices  103 us (51%)
  blocking collectives  31.1 us (15%)
  starting transfers between devices  21 us (10%)
  matrix products  21 us (10%)
  Pallas kernels  12.8 us (6%)
  local copies, waits for them, and re-layouts  6.43 us (3%)
  other arithmetic  5.15 us (3%)
    ppermute x1, waiting for transfers between devices, on_device(): home = lax.ppermute(far_sum.astype(BF16), 'ep', across)  46 us
    ppermute x1, waiting for transfers between devices, on_device(): far_normed = lax.ppermute(normed, 'ep', across)  38 us
    all_to_all x1, blocking collectives, exchange(): lax.all_to_all(array, 'ep', split_axis=0, concat_axis=0, tiled=True, axis...  31.1 us
    all_to_all x3, waiting for transfers between devices, exchange(): lax.all_to_all(array, 'ep', split_axis=0, concat_axis=0, tiled=True, axis...  19.1 us
    dot_general x6, matrix products, dot(): return jnp.dot(a, b, preferred_element_type=F32)  14.1 us
    all_to_all x3, starting transfers between devices, exchange(): lax.all_to_all(array, 'ep', split_axis=0, concat_axis=0, tiled=True, axis...  13.8 us
    pallas_call x2, Pallas kernels, expert(): pl.pallas_call(functools.partial(expert_kernel, parts=parts), out_shape=j...  12.8 us
    dot_general x2, matrix products, combine(): return lax.dot_general(weights, back, dims, preferred_element_type=F32)  6.95 us
  transfers between devices with their start and end apart: 9, of which 4 were waited for; matrix products, arithmetic and copies ran while one was open for 7% of the time, Pallas kernels for 3%

commit v1 on v0

--- a/solution.py
+++ b/solution.py
@@ -39,34 +39,43 @@
     return lax.dot_general(weights, back, dims, preferred_element_type=F32)
 
 
-def expert_kernel(*refs, parts):
-    x_ref, out_ref = refs[0], refs[-1]
-    x = x_ref[...]
+def expert_kernel(*refs, chunks, parts):
+    xs, weights, outs = refs[:chunks], refs[chunks:-chunks], refs[-chunks:]
+    span = xs[0].shape[1]
+
+    def project(ref):
+        total = None
+        for c in range(chunks):
+            piece = dot(xs[c][...], ref[c * span : (c + 1) * span, :])
+            total = piece if total is None else total + piece
+        return total
+
     hidden = []
     for p in range(parts):
-        gate = dot(x, refs[1 + p][...])
-        up = dot(x, refs[1 + parts + p][...])
+        gate, up = project(weights[p]), project(weights[parts + p])
         hidden.append((jax.nn.silu(gate) * up).astype(BF16))
-    width = out_ref.shape[1]
-    step = 256 if width % 256 == 0 else width
-    for at in range(0, width, step):
-        total = None
-        for p in range(parts):
-            piece = dot(hidden[p], refs[1 + 2 * parts + p][:, at : at + step])
-            total = piece if total is None else total + piece
-        out_ref[:, at : at + step] = total.astype(BF16)
-
-
-def expert(x, gate_parts, up_parts, down_parts):
-    parts = len(gate_parts)
-    rows, width = x.shape
+    step = 256 if span % 256 == 0 else span
+    for c in range(chunks):
+        for at in range(0, span, step):
+            total = None
+            for p in range(parts):
+                low = c * span + at
+                piece = dot(hidden[p], weights[2 * parts + p][:, low : low + step])
+                total = piece if total is None else total + piece
+            outs[c][:, at : at + step] = total.astype(BF16)
+
+
+def expert(xs, gate_parts, up_parts, down_parts):
+    parts, chunks = len(gate_parts), len(xs)
+    rows, span = xs[0].shape
+    width = span * chunks
     units = gate_parts[0].shape[1]
-    operands = [x, *gate_parts, *up_parts, *down_parts]
+    operands = [*xs, *gate_parts, *up_parts, *down_parts]
     return pl.pallas_call(
-        functools.partial(expert_kernel, parts=parts),
-        out_shape=jax.ShapeDtypeStruct((rows, width), BF16),
+        functools.partial(expert_kernel, chunks=chunks, parts=parts),
+        out_shape=[jax.ShapeDtypeStruct((rows, span), BF16)] * chunks,
         in_specs=[pl.BlockSpec(memory_space=pltpu.VMEM)] * len(operands),
-        out_specs=pl.BlockSpec(memory_space=pltpu.VMEM),
+        out_specs=[pl.BlockSpec(memory_space=pltpu.VMEM)] * chunks,
         cost_estimate=pl.CostEstimate(
             flops=6 * rows * width * units * parts,
             bytes_accessed=4 * rows * width + 6 * parts * width * units,
@@ -106,7 +115,14 @@
     scaling = lax.rsqrt(jnp.mean(values * values, axis=1, keepdims=True) + 1e-06)
     normed = (values * scaling * norm_gain[None, :]).astype(BF16)
 
-    far_normed = lax.ppermute(normed, "ep", across)
+    def columns(array):
+        return [array[..., c * span : (c + 1) * span] for c in range(chunks)]
+
+    chunks = 2 if width % 512 == 0 else 1
+    span = width // chunks
+    far_normed = []
+    for piece in columns(normed):
+        far_normed.append(lax.ppermute(piece, "ep", across))
     table = jnp.concatenate([routes.astype(F32), gates], axis=1)
     far_table = lax.ppermute(table, "ep", across)
     far_routes = far_table[:, :top].astype(jnp.int32)
@@ -126,15 +142,18 @@
 
     def send(onehot, source):
         picked = dot(onehot.astype(BF16), source).astype(BF16)
-        return exchange(picked.reshape(half, local, capacity, width))
+        return exchange(picked.reshape(half, local, capacity, source.shape[1]))
 
     def run(received):
         outs = []
         for e in range(local):
-            x = received[:, e].reshape(half * capacity, width)
+            xs = [piece[:, e].reshape(half * capacity, -1) for piece in received]
             weights = ([part[e] for part in kind] for kind in (gate_parts, up_parts, down_parts))
-            outs.append(expert(x, *weights).reshape(half, capacity, width))
-        return jnp.stack(outs, axis=1)
+            outs.append([o.reshape(half, capacity, -1) for o in expert(xs, *weights)])
+        return [jnp.stack([out[c] for out in outs], axis=1) for c in range(len(received))]
+
+    def flat(back):
+        return back.reshape(mine * capacity, back.shape[-1])
 
     near_slots = slots_of(routes, first, mine, capacity)
     near_in = send(near_slots, normed)
@@ -144,23 +163,38 @@
     ).astype(BF16)
     shared_out = dot(shared_hidden, shared_down)
     far_slots = slots_of(far_routes, first, mine, capacity).astype(BF16)
-    far_normed, near_in, shared_out, far_slots, far_gates, gate_parts, up_parts, down_parts = (
-        lax.optimization_barrier(
-            (far_normed, near_in, shared_out, far_slots, far_gates, gate_parts, up_parts, down_parts)
-        )
+    far_normed[0], near_in, shared_out, far_slots, far_gates = lax.optimization_barrier(
+        (far_normed[0], near_in, shared_out, far_slots, far_gates)
     )
-    far_in = send(far_slots, far_normed)
-    near_done = run(near_in)
+    far_in = []
+    for c in range(chunks):
+        if c:
+            far_normed[c], far_in[-1] = lax.optimization_barrier((far_normed[c], far_in[-1]))
+        far_in.append(send(far_slots, far_normed[c]))
+        if c == 0:
+            far_in[0], gate_parts, up_parts, down_parts = lax.optimization_barrier(
+                (far_in[0], gate_parts, up_parts, down_parts)
+            )
+    (near_done,) = run([near_in])
     near_weights = weights_of(near_slots, routes, gates, first, mine, capacity)
     far_weights = weights_of(far_slots > 0, far_routes, far_gates, first, mine, capacity)
-    far_in, near_done = lax.optimization_barrier((far_in, near_done))
-    far_back = exchange(run(far_in))
-    far_back, near_done = lax.optimization_barrier((far_back, near_done))
-    near_back = exchange(near_done).reshape(mine * capacity, width)
-    far_sum = combine(far_weights, far_back.reshape(mine * capacity, width))
-    home = lax.ppermute(far_sum.astype(BF16), "ep", across)
-    near_back, home = lax.optimization_barrier((near_back, home))
-    return (combine(near_weights, near_back) + (shared_out + home.astype(F32))).astype(BF16)
+    far_in, near_done, near_weights, far_weights = lax.optimization_barrier(
+        (far_in, near_done, near_weights, far_weights)
+    )
+    far_done = run(far_in)
+    homes = []
+    for c in range(chunks):
+        back = exchange(far_done[c])
+        far_sum = combine(far_weights, flat(back)).astype(BF16)
+        if c + 1 < chunks:
+            far_sum, far_done[c + 1] = lax.optimization_barrier((far_sum, far_done[c + 1]))
+        else:
+            far_sum, near_done = lax.optimization_barrier((far_sum, near_done))
+        homes.append(lax.ppermute(far_sum, "ep", across))
+    near_back = exchange(near_done)
+    near_back, homes = lax.optimization_barrier((near_back, homes))
+    home = jnp.concatenate(homes, axis=1)
+    return (combine(near_weights, flat(near_back)) + (shared_out + home.astype(F32))).astype(BF16)
 
 
 def solution(mesh):

time: 202 us -> 221 us (1.094)
  local copies, waits for them, and re-layouts: 6.43 us -> 20.3 us
  starting transfers between devices: 21 us -> 27.2 us
  waiting for transfers between devices: 103 us -> 97.4 us
  blocking collectives: 31.1 us -> 35.3 us
  other arithmetic: 5.15 us -> 7.57 us
    unnamed x20 -> x46, local copies, waits for them, and re-layouts: 6.32 us -> 19.1 us
    ppermute x2 -> x4, waiting for transfers between devices: 84 us -> 73.3 us  [the longest x2 41.9 us: on_device(): homes.append(lax.ppermute(far_sum, 'ep', across))]
    all_to_all x1 -> x2, blocking collectives: 31.1 us -> 35.3 us  [exchange(): lax.all_to_all(array, 'ep', split_axis=0, concat_axis=0, tiled=True, axis...]
    all_to_all x3 -> x4, starting transfers between devices: 13.8 us -> 16.9 us  [exchange(): lax.all_to_all(array, 'ep', split_axis=0, concat_axis=0, tiled=True, axis...]
    ppermute x2 -> x4, starting transfers between devices: 2.61 us -> 5.51 us  [the longest x2 2.99 us: on_device(): homes.append(lax.ppermute(far_sum, 'ep', across))]
    all_to_all x3 -> x4, waiting for transfers between devices: 19.1 us -> 22 us  [exchange(): lax.all_to_all(array, 'ep', split_axis=0, concat_axis=0, tiled=True, axis...]
    select_n x1 -> x2, other arithmetic: 0.14 us -> 2.57 us  [weights_of(): return jnp.where(onehot, wide, jnp.zeros((), BF16))]
    dot_general x6 -> x7, matrix products: 14.1 us -> 13.8 us  [dot(): return jnp.dot(a, b, preferred_element_type=F32)]
  transfers between devices with their start and end apart: 9 -> 12, of which waited for: 4 -> 10; matrix products, arithmetic and copies ran while one was open for 7% -> 6% of each run, Pallas kernels for 3% -> 3%
where the time goes in v1:
time: 221 us; the launch traced here: 219 us
  waiting for transfers between devices  97.4 us (44%)
  blocking collectives  35.3 us (16%)
  starting transfers between devices  27.2 us (12%)
  matrix products  20.9 us (9%)
  local copies, waits for them, and re-layouts  20.3 us (9%)
  Pallas kernels  10.6 us (5%)
  other arithmetic  7.57 us (3%)
    ppermute x2, waiting for transfers between devices, on_device(): homes.append(lax.ppermute(far_sum, 'ep', across))  41.9 us
    all_to_all x2, blocking collectives, exchange(): lax.all_to_all(array, 'ep', split_axis=0, concat_axis=0, tiled=True, axis...  35.3 us
    ppermute x2, waiting for transfers between devices, on_device(): far_normed.append(lax.ppermute(piece, 'ep', across))  31.4 us
    all_to_all x4, waiting for transfers between devices, exchange(): lax.all_to_all(array, 'ep', split_axis=0, concat_axis=0, tiled=True, axis...  22 us
    unnamed x46, local copies, waits for them, and re-layouts  19.1 us
    all_to_all x4, starting transfers between devices, exchange(): lax.all_to_all(array, 'ep', split_axis=0, concat_axis=0, tiled=True, axis...  16.9 us
    dot_general x7, matrix products, dot(): return jnp.dot(a, b, preferred_element_type=F32)  13.8 us
    pallas_call x2, Pallas kernels, expert(): pl.pallas_call(functools.partial(expert_kernel, chunks=chunks, parts=part...  10.6 us
  transfers between devices with their start and end apart: 12, of which 10 were waited for; matrix products, arithmetic and copies ran while one was open for 6% of the time, Pallas kernels for 3%

profile of v1, /device:TPU:0, one launch (start us, length us, event | category | flops | bytes accessed | tf_op | source)
XLA Modules:
  0.0 219.3 jit_solution(11131672780487658489)
XLA Ops:
  0.0 0.9 convert_element_type.69
  0.9 0.7 pad_maximum_fusion
  1.6 4.1 %collective-permute-start.2 = (f32[256,6]{0,1:T(8,128)S(1)}, f32[256,6]{0,1:T(8,128)S(1)}, u32[]{:S(2)}, u32[]{:S(2)}) collective-permute-start(f32[256,6]{0,1:T(8,128)S(1)} %pad_maximum_fusion), channel_id=1, source_target_pairs={{0,8},{2,10},{4,12},{6,14},{8,0},{10,2},{12,4},{14,6},{1,9},{3,11}... | collective-permute-start | bytes 18440 | tf_op jit(solution)/shard_map/ppermute | solution.py:127
  5.6 1.5 fusion.1
  7.2 1.5 fusion.3
  8.7 0.1 eq.84
  8.8 0.1 compare_reduce_fusion
  8.9 0.2 fusion.7
  9.1 0.2 fusion.6
  9.3 0.2 fusion.8
  9.5 2.2 %convolution_convert_fusion = bf16[576,2048]{1,0:T(8,128)(2,1)} fusion(pred[576,256]{1,0:T(32,128)(4,1)S(1)} %get-tuple-element.70, bf16[256,2048]{1,0:T(8,128)(2,1)S(1)} %fusion.3), kind=kOutput, calls=%fused_computation | convolution fusion | flops 605159424 | bytes 3555328 | tf_op jit(solution)/shard_map/dot_general | solution.py:15
  11.7 4.5 %all-to-all-start = ((bf16[4,1,144,2048]{3,2,1,0:T(8,128)(2,1)}), bf16[4,1,144,2048]{3,2,1,0:T(8,128)(2,1)}, u32[]{:S(2)}, u32[]{:S(2)}) async-start(bf16[4,1,144,2048]{3,2,1,0:T(8,128)(2,1)} %bitcast.85), calls=%async_computation | async-start | bytes 4718592 | tf_op jit(solution)/shard_map/all_to_all | solution.py:139
  16.2 0.0 copy-start.22
  16.2 1.1 fusion.18
  17.3 1.4 collective-permute-start.1
  18.7 1.5 fusion.20
  20.2 4.4 %fusion.5 = f32[256,2048]{1,0:T(8,128)} fusion(bf16[512,2048]{1,0:T(8,128)(2,1)S(1)} %copy-done, bf16[256,2048]{1,0:T(8,128)(2,1)S(1)} %fusion.3, bf16[2048,512]{1,0:T(8,128)(2,1)} %param.18, f32[256,512]{1,0:T(8,128)} %fusion.20), kind=kOutput, calls=%fused_computation.14 | convolution fusion | flops 1074528256 | bytes 7864320 | tf_op jit(solution)/shard_map/dot_general | solution.py:15
  24.6 28.5 %collective-permute-done.1 = bf16[256,1024]{1,0:T(8,128)(2,1)} collective-permute-done((bf16[256,1024]{1,0:T(8,128)(2,1)}, bf16[256,1024]{1,0:T(8,128)(2,1)}, u32[]{:S(2)}, u32[]{:S(2)}) %collective-permute-start.1) | collective-permute-done | bytes 524320 | tf_op jit(solution)/shard_map/ppermute | solution.py:125
  53.0 2.2 %all-to-all-done = bf16[4,1,144,2048]{3,2,1,0:T(8,128)(2,1)} async-done(((bf16[4,1,144,2048]{3,2,1,0:T(8,128)(2,1)}), bf16[4,1,144,2048]{3,2,1,0:T(8,128)(2,1)}, u32[]{:S(2)}, u32[]{:S(2)}) %all-to-all-start) | async-done | bytes 2359328 | tf_op jit(solution)/shard_map/all_to_all | solution.py:139
  55.3 2.6 %convolution_convert_fusion.2 = bf16[576,1024]{1,0:T(8,128)(2,1)} fusion(bf16[576,256]{1,0:T(8,128)(2,1)S(1)} %get-tuple-element.33, bf16[256,1024]{1,0:T(8,128)(2,1)} %collective-permute-done.1), kind=kOutput, calls=%fused_computation.9 | convolution fusion | flops 302579712 | bytes 1998848 | tf_op jit(solution)/shard_map/dot_general | solution.py:15
  57.9 3.5 %all-to-all-start.1 = ((bf16[4,1,144,1024]{3,2,1,0:T(8,128)(2,1)}), bf16[4,1,144,1024]{3,2,1,0:T(8,128)(2,1)S(1)}, u32[]{:S(2)}, u32[]{:S(2)}) async-start(bf16[4,1,144,1024]{3,2,1,0:T(8,128)(2,1)} %bitcast.86), calls=%async_computation.1 | async-start | bytes 2359296 | tf_op jit(solution)/shard_map/all_to_all | solution.py:139
  61.4 0.1 collective-permute-start.3
  61.5 0.5 collective-permute-start.4
  62.0 0.1 collective-permute-start.5
  62.1 1.2 collective-permute-start
  63.3 1.1 collective-permute-done.3
  64.4 1.0 copy-done.8
  65.3 0.5 collective-permute-done.4
  65.9 1.0 copy-done.11
  66.9 0.5 collective-permute-done.5
  67.4 1.0 copy-done.14
  68.3 17.6 %all-to-all-done.1 = bf16[4,1,144,1024]{3,2,1,0:T(8,128)(2,1)S(1)} async-done(((bf16[4,1,144,1024]{3,2,1,0:T(8,128)(2,1)}), bf16[4,1,144,1024]{3,2,1,0:T(8,128)(2,1)S(1)}, u32[]{:S(2)}, u32[]{:S(2)}) %all-to-all-start.1) | async-done | bytes 1179680 | tf_op jit(solution)/shard_map/all_to_all | solution.py:139
  85.9 2.9 %collective-permute-done = bf16[256,1024]{1,0:T(8,128)(2,1)} collective-permute-done((bf16[256,1024]{1,0:T(8,128)(2,1)}, bf16[256,1024]{1,0:T(8,128)(2,1)}, u32[]{:S(2)}, u32[]{:S(2)}) %collective-permute-start) | collective-permute-done | bytes 524320 | tf_op jit(solution)/shard_map/ppermute | solution.py:125
  88.8 2.7 %convolution_convert_fusion.1 = bf16[576,1024]{1,0:T(8,128)(2,1)} fusion(bf16[576,256]{1,0:T(8,128)(2,1)} %copy-done.17, bf16[256,1024]{1,0:T(8,128)(2,1)} %collective-permute-done), kind=kOutput, calls=%fused_computation.8 | convolution fusion | flops 302579712 | bytes 1998848 | tf_op jit(solution)/shard_map/dot_general | solution.py:15
  91.6 4.3 %all-to-all-start.2 = ((bf16[4,1,144,1024]{3,2,1,0:T(8,128)(2,1)}), bf16[4,1,144,1024]{3,2,1,0:T(8,128)(2,1)}, u32[]{:S(2)}, u32[]{:S(2)}) async-start(bf16[4,1,144,1024]{3,2,1,0:T(8,128)(2,1)} %bitcast.87), calls=%async_computation.2 | async-start | bytes 2359296 | tf_op jit(solution)/shard_map/all_to_all | solution.py:139
  95.8 0.1 fusion.16
  95.9 0.9 bitcast_select_fusion
  96.8 1.7 compare_select_fusion
  98.5 1.2 copy-done.2
  99.7 1.2 copy-done.4
  101.0 1.2 copy-done.6
  102.2 1.2 copy-done.9
  103.4 1.2 copy-done.12
  104.6 1.2 copy-done.15
  105.9 5.5 %expert.2 = bf16[576,2048]{1,0:T(8,128)(2,1)S(1)} custom-call(bf16[576,2048]{1,0:T(8,128)(2,1)} %bitcast.10.refs_0_, bf16[2048,256]{1,0:T(8,128)(2,1)S(1)} %bitcast.73, bf16[2048,256]{1,0:T(8,128)(2,1)S(1)} %bitcast.79, bf16[2048,256]{1,0:T(8,128)(2,1)S(1)} %bitcast.75, bf16[2048,256]{1,0:T(8,128)(2,1)S(1)} %bitcast.81, bf16[256,2048]{1,0:T(8,128)(2,1)S(1)} %bitcast.77, ...), custom_call_target="tpu_custom_call" | custom-call | flops 3623878656 | bytes 11010048 | tf_op jit(solution)/shard_map/expert/pallas_call | solution.py:74
  111.4 1.4 copy-done.1
  112.8 1.2 copy-done.3
  114.0 1.2 copy-done.5
  115.2 1.2 copy-done.7
  116.4 1.2 copy-done.10
  117.7 1.2 copy-done.13
  118.9 1.2 copy-done.16
  120.1 5.1 %expert.3 = (bf16[576,1024]{1,0:T(8,128)(2,1)S(1)}, bf16[576,1024]{1,0:T(8,128)(2,1)S(1)}) custom-call(bf16[576,1024]{1,0:T(8,128)(2,1)S(1)} %bitcast.70, bf16[576,1024]{1,0:T(8,128)(2,1)} %bitcast.23.refs_1_, bf16[2048,256]{1,0:T(8,128)(2,1)S(1)} %bitcast.74, bf16[2048,256]{1,0:T(8,128)(2,1)S(1)} %bitcast.80, bf16[2048,256]{1,0:T(8,128)(2,1)S(1)} %bitcast.76, ...), custom_call_target="tpu_custom_call" | custom-call | flops 3623878656 | bytes 11010048 | tf_op jit(solution)/shard_map/expert/pallas_call | solution.py:74
  125.2 19.1 %all_to_all.30 = bf16[4,1,144,1024]{3,2,1,0:T(8,128)(2,1)S(1)} all-to-all(bf16[4,1,144,1024]{3,2,1,0:T(8,128)(2,1)S(1)} %bitcast.72), channel_id=1, replica_groups={{0,2,4,6},{8,10,12,14},{1,3,5,7},{9,11,13,15},{16,18,20,22},{24,26,28,3..., dimensions={0} | all-to-all | bytes 2359296 | tf_op jit(solution)/shard_map/all_to_all | solution.py:139
  144.3 1.4 convolution_convert_fusion.4
  145.7 16.2 %all_to_all.31 = bf16[4,1,144,1024]{3,2,1,0:T(8,128)(2,1)S(1)} all-to-all(bf16[4,1,144,1024]{3,2,1,0:T(8,128)(2,1)S(1)} %bitcast.71), channel_id=1, replica_groups={{0,2,4,6},{8,10,12,14},{1,3,5,7},{9,11,13,15},{16,18,20,22},{24,26,28,3..., dimensions={0} | all-to-all | bytes 2359296 | tf_op jit(solution)/shard_map/all_to_all | solution.py:139
  161.9 1.4 convolution_convert_fusion.3
  163.3 4.7 %all-to-all-start.5 = ((bf16[4,1,144,2048]{3,2,1,0:T(8,128)(2,1)}), bf16[4,1,144,2048]{3,2,1,0:T(8,128)(2,1)}, u32[]{:S(2)}, u32[]{:S(2)}) async-start(bf16[4,1,144,2048]{3,2,1,0:T(8,128)(2,1)} %bitcast.69), calls=%async_computation.5 | async-start | bytes 4718592 | tf_op jit(solution)/shard_map/all_to_all | solution.py:139
  168.0 2.0 collective-permute-start.6
  169.9 1.0 collective-permute-start.7
  171.0 34.9 %collective-permute-done.6 = bf16[256,1024]{1,0:T(8,128)(2,1)S(1)} collective-permute-done((bf16[256,1024]{1,0:T(8,128)(2,1)}, bf16[256,1024]{1,0:T(8,128)(2,1)S(1)}, u32[]{:S(2)}, u32[]{:S(2)}) %collective-permute-start.6) | collective-permute-done | bytes 524320 | tf_op jit(solution)/shard_map/ppermute | solution.py:193
  205.9 7.0 %collective-permute-done.7 = bf16[256,1024]{1,0:T(8,128)(2,1)S(1)} collective-permute-done((bf16[256,1024]{1,0:T(8,128)(2,1)}, bf16[256,1024]{1,0:T(8,128)(2,1)S(1)}, u32[]{:S(2)}, u32[]{:S(2)}) %collective-permute-start.7) | collective-permute-done | bytes 524320 | tf_op jit(solution)/shard_map/ppermute | solution.py:193
  212.8 2.2 %all-to-all-done.5 = bf16[4,1,144,2048]{3,2,1,0:T(8,128)(2,1)} async-done(((bf16[4,1,144,2048]{3,2,1,0:T(8,128)(2,1)}), bf16[4,1,144,2048]{3,2,1,0:T(8,128)(2,1)}, u32[]{:S(2)}, u32[]{:S(2)}) %all-to-all-start.5) | async-done | bytes 2359328 | tf_op jit(solution)/shard_map/all_to_all | solution.py:139
  215.0 4.3 %fusion = bf16[256,2048]{1,0:T(8,128)(2,1)} fusion(bf16[576,256]{1,0:T(8,128)(2,1)S(1)} %copy-done.18, bf16[576,2048]{1,0:T(8,128)(2,1)} %bitcast.31, f32[256,2048]{1,0:T(8,128)} %fusion.5, bf16[256,1024]{1,0:T(8,128)(2,1)S(1)} %collective-permute-done.7, bf16[256,1024]{1,0:T(8,128)(2,1)S(1)} %collective-permute-done.6), kind=kOutput, calls=%fused_computation.4 | convolution fusion | flops 607649792 | bytes 6848512 | tf_op jit(solution)/shard_map/dot_general | solution.py:39
  (35 shorter events, 0.1 us)
Async XLA Ops:
  0.0 20.2 %copy-start = (bf16[512,2048]{1,0:T(8,128)(2,1)S(1)}, bf16[512,2048]{1,0:T(8,128)(2,1)}, u32[]{:S(2)}) copy-start(bf16[512,2048]{1,0:T(8,128)(2,1)} %param.19) | copy-start | bytes 6291460
  0.0 8.8 %copy-start.20 = (s32[256,3]{0,1:T(4,128)S(1)}, s32[256,3]{0,1:T(4,128)}, u32[]{:S(2)}) copy-start(s32[256,3]{0,1:T(4,128)} %param.12) | copy-start | bytes 9220
  1.6 7.2 %collective-permute-start.2 = (f32[256,6]{0,1:T(8,128)S(1)}, f32[256,6]{0,1:T(8,128)S(1)}, u32[]{:S(2)}, u32[]{:S(2)}) collective-permute-start(f32[256,6]{0,1:T(8,128)S(1)} %pad_maximum_fusion), channel_id=1, source_target_pairs={{0,8},{2,10},{4,12},{6,14},{8,0},{10,2},{12,4},{14,6},{1,9},{3,11}... | collective-permute-start | bytes 18440 | tf_op jit(solution)/shard_map/ppermute | solution.py:127
  9.5 45.8 %copy-start.17 = (bf16[576,256]{1,0:T(8,128)(2,1)}, bf16[576,256]{1,0:T(8,128)(2,1)S(1)}, u32[]{:S(2)}) copy-start(bf16[576,256]{1,0:T(8,128)(2,1)S(1)} %get-tuple-element.33) | copy-start | bytes 884740
  11.7 43.5 %all-to-all-start = ((bf16[4,1,144,2048]{3,2,1,0:T(8,128)(2,1)}), bf16[4,1,144,2048]{3,2,1,0:T(8,128)(2,1)}, u32[]{:S(2)}, u32[]{:S(2)}) async-start(bf16[4,1,144,2048]{3,2,1,0:T(8,128)(2,1)} %bitcast.85), calls=%async_computation | async-start | bytes 4718592 | tf_op jit(solution)/shard_map/all_to_all | solution.py:139
  16.2 2.5 %copy-start.22 = (bf16[2048,512]{1,0:T(8,128)(2,1)S(1)}, bf16[2048,512]{1,0:T(8,128)(2,1)}, u32[]{:S(2)}) copy-start(bf16[2048,512]{1,0:T(8,128)(2,1)} %param.17) | copy-start | bytes 6291460
  17.3 35.7 %collective-permute-start.1 = (bf16[256,1024]{1,0:T(8,128)(2,1)}, bf16[256,1024]{1,0:T(8,128)(2,1)}, u32[]{:S(2)}, u32[]{:S(2)}) collective-permute-start(bf16[256,1024]{1,0:T(8,128)(2,1)} %get-tuple-element.65), channel_id=1, source_target_pairs={{0,8},{2,10},{4,12},{6,14},{8,0},{10,2},{12,4},{14,6},{1,9},{3,11}... | collective-permute-start | bytes 1572872 | tf_op jit(solution)/shard_map/ppermute | solution.py:125
  57.9 28.0 %all-to-all-start.1 = ((bf16[4,1,144,1024]{3,2,1,0:T(8,128)(2,1)}), bf16[4,1,144,1024]{3,2,1,0:T(8,128)(2,1)S(1)}, u32[]{:S(2)}, u32[]{:S(2)}) async-start(bf16[4,1,144,1024]{3,2,1,0:T(8,128)(2,1)} %bitcast.86), calls=%async_computation.1 | async-start | bytes 2359296 | tf_op jit(solution)/shard_map/all_to_all | solution.py:139
  61.4 2.9 %collective-permute-start.3 = (bf16[1,2048,256]{2,1,0:T(8,128)(2,1)}, bf16[1,2048,256]{2,1,0:T(8,128)(2,1)S(1)}, u32[]{:S(2)}, u32[]{:S(2)}) collective-permute-start(bf16[1,2048,256]{2,1,0:T(8,128)(2,1)} %param.14), channel_id=1, source_target_pairs={{0,1},{1,0},{2,3},{3,2},{4,5},{5,4},{6,7},{7,6},{8,9},{9,8},{10,11... | collective-permute-start | bytes 3145736 | tf_op jit(solution)/shard_map/ppermute | solution.py:134
  61.5 4.4 %collective-permute-start.4 = (bf16[1,2048,256]{2,1,0:T(8,128)(2,1)}, bf16[1,2048,256]{2,1,0:T(8,128)(2,1)S(1)}, u32[]{:S(2)}, u32[]{:S(2)}) collective-permute-start(bf16[1,2048,256]{2,1,0:T(8,128)(2,1)} %param.15), channel_id=1, source_target_pairs={{0,1},{1,0},{2,3},{3,2},{4,5},{5,4},{6,7},{7,6},{8,9},{9,8},{10,11... | collective-permute-start | bytes 3145736 | tf_op jit(solution)/shard_map/ppermute | solution.py:135
  62.0 5.4 %collective-permute-start.5 = (bf16[1,256,2048]{2,1,0:T(8,128)(2,1)}, bf16[1,256,2048]{2,1,0:T(8,128)(2,1)S(1)}, u32[]{:S(2)}, u32[]{:S(2)}) collective-permute-start(bf16[1,256,2048]{2,1,0:T(8,128)(2,1)} %param.16), channel_id=1, source_target_pairs={{0,1},{1,0},{2,3},{3,2},{4,5},{5,4},{6,7},{7,6},{8,9},{9,8},{10,11... | collective-permute-start | bytes 3145736 | tf_op jit(solution)/shard_map/ppermute | solution.py:136
  62.1 33.7 %copy-start.21 = (f32[256,3]{0,1:T(4,128)S(1)}, f32[256,3]{0,1:T(4,128)}, u32[]{:S(2)}) copy-start(f32[256,3]{0,1:T(4,128)} %param.13) | copy-start | bytes 9220
  62.1 26.8 %collective-permute-start = (bf16[256,1024]{1,0:T(8,128)(2,1)}, bf16[256,1024]{1,0:T(8,128)(2,1)}, u32[]{:S(2)}, u32[]{:S(2)}) collective-permute-start(bf16[256,1024]{1,0:T(8,128)(2,1)} %get-tuple-element.66), channel_id=1, source_target_pairs={{0,8},{2,10},{4,12},{6,14},{8,0},{10,2},{12,4},{14,6},{1,9},{3,11}... | collective-permute-start | bytes 1572872 | tf_op jit(solution)/shard_map/ppermute | solution.py:125
  64.4 1.0 copy-start.8
  65.9 1.0 copy-start.11
  67.4 1.0 copy-start.14
  91.6 21.2 %all-to-all-start.2 = ((bf16[4,1,144,1024]{3,2,1,0:T(8,128)(2,1)}), bf16[4,1,144,1024]{3,2,1,0:T(8,128)(2,1)}, u32[]{:S(2)}, u32[]{:S(2)}) async-start(bf16[4,1,144,1024]{3,2,1,0:T(8,128)(2,1)} %bitcast.87), calls=%async_computation.2 | async-start | bytes 2359296 | tf_op jit(solution)/shard_map/all_to_all | solution.py:139
  98.5 1.2 copy-start.2
  99.7 1.2 copy-start.4
  101.0 1.2 copy-start.6
  102.2 1.2 copy-start.9
  103.4 1.2 copy-start.12
  104.6 1.2 copy-start.15
  111.3 1.4 copy-start.1
  112.8 1.2 copy-start.3
  114.0 1.2 copy-start.5
  115.2 1.2 copy-start.7
  116.4 1.2 copy-start.10
  117.7 1.2 copy-start.13
  118.9 1.2 copy-start.16
  125.2 19.1 %copy-start.19 = (bf16[576,256]{1,0:T(8,128)(2,1)S(1)}, bf16[576,256]{1,0:T(8,128)(2,1)}, u32[]{:S(2)}) copy-start(bf16[576,256]{1,0:T(8,128)(2,1)} %compare_select_fusion) | copy-start | bytes 884740
  163.3 51.7 %copy-start.18 = (bf16[576,256]{1,0:T(8,128)(2,1)S(1)}, bf16[576,256]{1,0:T(8,128)(2,1)}, u32[]{:S(2)}) copy-start(bf16[576,256]{1,0:T(8,128)(2,1)} %bitcast_select_fusion) | copy-start | bytes 884740
  163.3 51.7 %all-to-all-start.5 = ((bf16[4,1,144,2048]{3,2,1,0:T(8,128)(2,1)}), bf16[4,1,144,2048]{3,2,1,0:T(8,128)(2,1)}, u32[]{:S(2)}, u32[]{:S(2)}) async-start(bf16[4,1,144,2048]{3,2,1,0:T(8,128)(2,1)} %bitcast.69), calls=%async_computation.5 | async-start | bytes 4718592 | tf_op jit(solution)/shard_map/all_to_all | solution.py:139
  168.0 37.9 %collective-permute-start.6 = (bf16[256,1024]{1,0:T(8,128)(2,1)}, bf16[256,1024]{1,0:T(8,128)(2,1)S(1)}, u32[]{:S(2)}, u32[]{:S(2)}) collective-permute-start(bf16[256,1024]{1,0:T(8,128)(2,1)} %convolution_convert_fusion.4), channel_id=1, source_target_pairs={{0,8},{2,10},{4,12},{6,14},{8,0},{10,2},{12,4},{14,6},{1,9},{3,11}... | collective-permute-start | bytes 1572872 | tf_op jit(solution)/shard_map/ppermute | solution.py:193
  169.9 42.9 %collective-permute-start.7 = (bf16[256,1024]{1,0:T(8,128)(2,1)}, bf16[256,1024]{1,0:T(8,128)(2,1)S(1)}, u32[]{:S(2)}, u32[]{:S(2)}) collective-permute-start(bf16[256,1024]{1,0:T(8,128)(2,1)} %convolution_convert_fusion.3), channel_id=1, source_target_pairs={{0,8},{2,10},{4,12},{6,14},{8,0},{10,2},{12,4},{14,6},{1,9},{3,11}... | collective-permute-start | bytes 1572872 | tf_op jit(solution)/shard_map/ppermute | solution.py:193
